TPU v7x, 256 devices: a whole 4x4x8 slice. The times are simulated.
256 devices in a mesh: sp: 64 (over z, y, core), tp: 4 (over x).
Axes of the slice: x: 4, y: 4, z: 8, core: 2. Of those that a mesh axis runs over, the one named last changes fastest.
Arguments:
- residual: bfloat16 [8192, 2048], P(('sp', 'tp')), may hold values from -6 to 6
- query_content: bfloat16 [8192, 1024], P('sp', 'tp'), may hold values from -400 to 400
- query_rotary: bfloat16 [8192, 384], P('sp', 'tp'), may hold values from -16 to 16
- key_latent: bfloat16 [8192, 512], P('sp'), may hold values from -6 to 6
- rotary_key: bfloat16 [8192, 32], P('sp'), may hold values from -6 to 6
- latent_gain: float32 [512], replicated, may hold values from 0.1 to 1.9
- key_weight: bfloat16 [512, 1024], P(None, 'tp'), may hold values from -0.25 to 0.25
- value_weight: bfloat16 [512, 1024], P(None, 'tp'), may hold values from -0.25 to 0.25
- output_gain: float32 [1024], P('tp'), may hold values from 0.1 to 1.9
- output_weight: bfloat16 [1024, 2048], P('tp'), may hold values from -0.1875 to 0.1875
- mixer_gain: float32 [2048], replicated, may hold values from 0.1 to 1.9
- gate_weight: bfloat16 [2048, 5632], P('sp', 'tp'), may hold values from -0.125 to 0.125
- up_weight: bfloat16 [2048, 5632], P('sp', 'tp'), may hold values from -0.125 to 0.125
- down_weight: bfloat16 [5632, 2048], P('tp', 'sp'), may hold values from -0.078125 to 0.078125
Outputs:
- layer_out: bfloat16 [8192, 2048], P(('sp', 'tp'))
All inputs are finite; a program needn't handle non-finite values.
Results may differ from a plain program's by a relative error of at most 0.015.
Values may be sent and summed in bfloat16 or wider, within the bound.
A program may use at most 128 MiB of HBM per device.

v0:
```python
import jax
import jax.numpy as jnp
from jax import lax
from jax.sharding import PartitionSpec as P

NARROW_HEADS = 8
WIDE_HEADS = 4
NARROW_DIM = 64
WIDE_DIM = 128
ROT_DIM = 32
epsilon = 1e-06
rope_base = 500000.0


def turned_gather(arrays, axis, dims):
    turned = [jnp.moveaxis(a, dim, 0) for a, dim in zip(arrays, dims)]
    both = jnp.concatenate([t.reshape(len(t), -1) for t in turned], axis=1)
    filled, at, done = (lax.all_gather(both, axis, axis=0, tiled=True), 0, [])
    for t, dim in zip(turned, dims):
        piece = filled[:, at : at + t[0].size].reshape(-1, *t.shape[1:])
        done.append(jnp.moveaxis(piece, 0, dim))
        at += t[0].size
    return tuple(done)


def side_by_side(arrays, axis, dim, along):
    widths = [a.shape[along] for a in arrays]
    both = jnp.concatenate(arrays, axis=along)
    filled = lax.all_gather(both, axis, axis=dim, tiled=True)
    return tuple(jnp.split(filled, [sum(widths[:k]) for k in range(1, len(widths))], axis=along))


def split_up(x, dim, size):
    before, after = (x.shape[:dim], x.shape[dim + 1 :])
    return jnp.moveaxis(x.reshape(*before, size, -1, *after), dim, 0)


def summed_on_arrival(x, axis, dim):
    pieces = split_up(x, dim, lax.axis_size(axis))
    arrived = lax.all_to_all(pieces, axis, split_axis=0, concat_axis=0, tiled=True)
    return arrived.astype(jnp.float32).sum(axis=0)


def normalize(values):
    values = values.astype(jnp.float32)
    return values * lax.rsqrt(jnp.mean(values * values, axis=-1, keepdims=True) + epsilon)


def rotate(values, positions):
    half_width = values.shape[-1] // 2
    inverse = 1.0 / jnp.power(
        rope_base, jnp.arange(0, 2 * half_width, 2, dtype=jnp.float32) / (2 * half_width)
    )
    angles = positions.astype(jnp.float32)[:, None] * inverse[None, :]
    table_shape = (angles.shape[0],) + (1,) * (values.ndim - 2) + (half_width,)
    cosine_table = jnp.cos(angles).reshape(table_shape)
    sine_table = jnp.sin(angles).reshape(table_shape)
    first_half = values[..., :half_width]
    second_half = values[..., half_width:]
    return jnp.concatenate(
        [
            first_half * cosine_table - second_half * sine_table,
            second_half * cosine_table + first_half * sine_table,
        ],
        axis=-1,
    )


def group_update(carried, query_part, rotary_part, key_part, rotary_keys, value_part, factor):
    running_max, totals, accumulated = carried
    scores = (
        jnp.einsum("qhd,khd->hqk", query_part, key_part, preferred_element_type=jnp.float32)
        + jnp.einsum("qhd,kd->hqk", rotary_part, rotary_keys, preferred_element_type=jnp.float32)
    ) * factor
    new_max = jnp.max(scores, axis=-1)
    shrink = jnp.exp(running_max - new_max)
    powers = jnp.exp(scores - new_max[..., None])
    totals = totals * shrink + jnp.sum(powers, axis=-1)
    added = jnp.einsum(
        "hqk,khd->qhd", powers.astype(jnp.bfloat16), value_part, preferred_element_type=jnp.float32
    )
    accumulated = accumulated * jnp.transpose(shrink)[:, :, None] + added
    return (new_max, totals, accumulated)


def on_device(
    residual,
    query_content,
    query_rotary,
    key_latent,
    rotary_key,
    latent_gain,
    key_weight,
    value_weight,
    output_gain,
    output_weight,
    mixer_gain,
    gate_weight,
    up_weight,
    down_weight,
):
    tp_count = lax.axis_size("tp")
    narrow_dev = NARROW_HEADS // tp_count
    wide_dev = WIDE_HEADS // tp_count
    row_count = key_latent.shape[0]
    gate_whole, up_whole, down_whole = turned_gather(
        (gate_weight, up_weight, down_weight), "sp", (0, 0, 1)
    )
    positions = lax.axis_index("sp") * row_count + lax.iota(jnp.int32, row_count)
    latent = (normalize(key_latent) * latent_gain).astype(jnp.bfloat16)
    key_rows = jnp.dot(latent, key_weight, preferred_element_type=jnp.float32).astype(jnp.bfloat16)
    value_rows = jnp.dot(latent, value_weight, preferred_element_type=jnp.float32).astype(
        jnp.bfloat16
    )
    rot_keys = rotate(rotary_key.astype(jnp.float32), positions).astype(jnp.bfloat16)
    head_count = narrow_dev + wide_dev
    rot_queries = rotate(
        query_rotary.astype(jnp.float32).reshape(row_count, head_count, ROT_DIM), positions
    ).astype(jnp.bfloat16)
    narrow_cols = narrow_dev * NARROW_DIM
    query_narrow = query_content[:, :narrow_cols].reshape(row_count, narrow_dev, NARROW_DIM)
    query_wide = query_content[:, narrow_cols:].reshape(row_count, wide_dev, WIDE_DIM)
    rotary_narrow = rot_queries[:, :narrow_dev]
    rotary_wide = rot_queries[:, narrow_dev:]
    narrow_factor = (NARROW_DIM + ROT_DIM) ** (-0.5)
    wide_factor = (WIDE_DIM + ROT_DIM) ** (-0.5)

    def start_state(count, width):
        return (
            jnp.full((count, row_count), -jnp.inf, jnp.float32),
            jnp.zeros((count, row_count), jnp.float32),
            jnp.zeros((row_count, count, width), jnp.float32),
        )

    carried = (start_state(narrow_dev, NARROW_DIM), start_state(wide_dev, WIDE_DIM))
    piece_keys, piece_rotary, piece_values = side_by_side(
        (key_rows, rot_keys, value_rows), "sp", 0, 1
    )
    length = piece_keys.shape[0]
    narrow_keys = piece_keys[:, :narrow_cols].reshape(length, narrow_dev, NARROW_DIM)
    wide_keys = piece_keys[:, narrow_cols:].reshape(length, wide_dev, WIDE_DIM)
    narrow_values = piece_values[:, :narrow_cols].reshape(length, narrow_dev, NARROW_DIM)
    wide_values = piece_values[:, narrow_cols:].reshape(length, wide_dev, WIDE_DIM)
    narrow_state = group_update(
        carried[0],
        query_narrow,
        rotary_narrow,
        narrow_keys,
        piece_rotary,
        narrow_values,
        narrow_factor,
    )
    wide_state = group_update(
        carried[1], query_wide, rotary_wide, wide_keys, piece_rotary, wide_values, wide_factor
    )
    narrow_state, wide_state = (narrow_state, wide_state)

    def finish(carried):
        return normalize(carried[2] / jnp.transpose(carried[1])[:, :, None]).reshape(row_count, -1)

    mixed = (
        jnp.concatenate([finish(narrow_state), finish(wide_state)], axis=1) * output_gain
    ).astype(jnp.bfloat16)
    projected = summed_on_arrival(
        jnp.dot(mixed, output_weight, preferred_element_type=jnp.float32).astype(jnp.bfloat16),
        "tp",
        0,
    )
    middle = (residual.astype(jnp.float32) + projected).astype(jnp.bfloat16)
    normed = (normalize(middle) * mixer_gain).astype(jnp.bfloat16)
    block_normed = lax.all_gather(normed, "tp", axis=0, tiled=True)
    gate_sums = jnp.dot(block_normed, gate_whole, preferred_element_type=jnp.float32)
    up_sums = jnp.dot(block_normed, up_whole, preferred_element_type=jnp.float32)
    hidden = (jax.nn.silu(gate_sums) * up_sums).astype(jnp.bfloat16)
    channel_out = summed_on_arrival(
        jnp.dot(hidden, down_whole, preferred_element_type=jnp.float32).astype(jnp.bfloat16),
        "tp",
        0,
    )
    return (middle.astype(jnp.float32) + channel_out).astype(jnp.bfloat16)


def solution(mesh):
    placed = (
        P(("sp", "tp"), None),
        P("sp", "tp"),
        P("sp", "tp"),
        P("sp", None),
        P("sp", None),
        P(),
        P(None, "tp"),
        P(None, "tp"),
        P("tp"),
        P("tp", None),
        P(),
        P("sp", "tp"),
        P("sp", "tp"),
        P("tp", "sp"),
    )
    return jax.shard_map(
        on_device, mesh=mesh, in_specs=placed, out_specs=P(("sp", "tp"), None), check_vma=False
    )
```

profile of v0, /device:TPU:1, one launch (start us, length us, event | category | flops | bytes accessed | tf_op | source)
XLA Modules:
  0.0 234.1 jit_solution(12337247251630548791)
XLA Ops:
  6.6 0.8 convert_element_type.70
  7.7 1.0 fusion.67
  8.8 1.3 convolution_convert_fusion.1
  10.0 1.3 convolution_convert_fusion.2
  11.3 0.8 pad_maximum_fusion.1
  12.2 1.7 pad_maximum_fusion
  15.6 86.9 %all-gather.3.cloned.1.call-done = bf16[8192,544]{1,0:T(8,128)(2,1)} async-done(((bf16[128,544]{1,0:T(8,128)(2,1)}), bf16[8192,544]{1,0:T(8,128)(2,1)}) %all-gather.3.cloned.1.call-update) | async-done | bytes 8912912 | tf_op jit(solution)/shard_map/all_gather | solution.py:29
  102.4 5.7 %fusion.90 = (bf16[8192,128]{1,0:T(8,128)(2,1)}, bf16[8192,128]{1,0:T(8,128)(2,1)}) fusion(bf16[8192,544]{1,0:T(8,128)(2,1)} %all-gather.3.cloned.1.call-done), kind=kLoop, calls=%fused_computation.99 | loop fusion | bytes 8388608 | tf_op jit(solution)/shard_map/slice | solution.py:140
  108.1 2.9 %copy.33 = bf16[8192,128]{0,1:T(8,128)(2,1)S(1)} copy(bf16[8192,128]{1,0:T(8,128)(2,1)} %get-tuple-element.7) | data formatting | bytes 4194304 | tf_op jit(solution)/shard_map/slice | solution.py:140
  111.0 4.1 %copy.36 = bf16[8192,128]{0,1:T(8,128)(2,1)} copy(bf16[8192,128]{1,0:T(8,128)(2,1)} %get-tuple-element.8) | data formatting | bytes 4194304 | tf_op jit(solution)/shard_map/slice | solution.py:142
  115.1 2.3 convolution_bitcast_fusion.2
  117.5 2.9 %fusion.91 = (f32[128]{0:T(128)S(1)}, f32[1,128,8192]{1,2,0:T(8,128)S(1)}) fusion(f32[1,128,8192]{1,2,0:T(8,128)S(1)} %convolution_bitcast_fusion.2, bf16[128,256]{1,0:T(8,128)(2,1)S(1)} %copy-done.3, bf16[8192,544]{1,0:T(8,128)(2,1)} %all-gather.3.cloned.1.call-done), kind=kOutput, calls=%fused_computation.100 | convolution fusion | flops 271581056 | bytes 10519040 | tf_op jit(solution)/shard_map/qhd,khd->hqk/dot_general | solution.py:72
  120.3 1.1 fusion.15
  121.4 3.9 %multiply_reduce_fusion = (f32[128]{0:T(128)S(1)}, f32[1,128,128]{2,1,0:T(8,128)S(1)}) fusion(f32[128]{0:T(128)S(1)} %get-tuple-element.18, f32[1,128,8192]{1,2,0:T(8,128)S(1)} %get-tuple-element.20, f32[128]{0:T(128)S(1)} %get-tuple-element.19, bf16[8192,544]{1,0:T(8,128)(2,1)} %all-gather.3.cloned.1.call-done, f32[128]{0:T(128)S(1)} %get-tuple-element.17), kind=kOutput, calls=%fused_computation.69 | convolution fusion | flops 270598016 | bytes 6359040 | tf_op jit(solution)/shard_map/hqk,khd->qhd/dot_general | solution.py:79
  125.3 2.8 %convolution_bitcast_fusion = f32[2,128,8192]{1,2,0:T(8,128)S(1)} fusion(bf16[8192,544]{1,0:T(8,128)(2,1)} %all-gather.3.cloned.1.call-done, bf16[128,3,16]{0,2,1:T(8,128)(2,1)S(1)} %get-tuple-element.9, bf16[128,3,16]{0,2,1:T(8,128)(2,1)S(1)} %get-tuple-element.10), kind=kOutput, calls=%fused_computation | convolution fusion | flops 134250496 | bytes 10510336 | tf_op jit(solution)/shard_map/qhd,kd->hqk/dot_general | solution.py:73
  128.2 2.1 fusion.92
  130.3 1.1 fusion.4
  131.9 1.6 multiply_reduce_fusion.1
  134.1 12.9 %all_to_all.10 = bf16[4,32,2048]{2,1,0:T(8,128)(2,1)S(1)} all-to-all(bf16[4,32,2048]{2,1,0:T(8,128)(2,1)S(1)} %bitcast.78), channel_id=1, replica_groups=mesh['sp'=64,'tp'=4] {'tp'}, dimensions={0} | all-to-all | bytes 1048576 | tf_op jit(solution)/shard_map/all_to_all | solution.py:40
  147.3 11.0 %all_gather.10 = bf16[128,2048]{1,0:T(8,128)(2,1)S(1)} all-gather(bf16[32,2048]{1,0:T(8,128)(2,1)S(1)} %fusion.72), channel_id=1, replica_groups=mesh['sp'=64,'tp'=4] {'tp'}, dimensions={0}, use_global_device_ids=true | all-gather | bytes 655360 | tf_op jit(solution)/shard_map/all_gather | solution.py:171
  158.3 44.5 %all-gather.5.cloned.1.call-done = bf16[2048,4224]{1,0:T(8,128)(2,1)} async-done(((bf16[32,4224]{1,0:T(8,128)(2,1)}), bf16[2048,4224]{1,0:T(8,128)(2,1)}) %all-gather.5.cloned.1.call-update) | async-done | bytes 17301520 | tf_op jit(solution)/shard_map/all_gather | solution.py:18
  202.8 3.6 %fusion.10 = f32[128,1408]{1,0:T(8,128)S(1)} fusion(bf16[128,2048]{1,0:T(8,128)(2,1)S(1)} %all_gather.10, bf16[2048,4224]{1,0:T(8,128)(2,1)} %all-gather.5.cloned.1.call-done), kind=kOutput, calls=%fused_computation.15 | convolution fusion | flops 738197504 | bytes 7012352 | tf_op jit(solution)/shard_map/dot_general | solution.py:172
  206.5 7.2 %fusion.20 = bf16[128,2048]{1,0:T(8,128)(2,1)S(1)} fusion(bf16[2048,4224]{1,0:T(8,128)(2,1)} %all-gather.5.cloned.1.call-done, bf16[128,2048]{1,0:T(8,128)(2,1)S(1)} %all_gather.10, f32[128,1408]{1,0:T(8,128)S(1)} %fusion.10), kind=kOutput, calls=%fused_computation.23 | convolution fusion | flops 1477738496 | bytes 13303808 | tf_op jit(solution)/shard_map/dot_general | solution.py:176
  213.7 12.8 %all_to_all.11 = bf16[4,32,2048]{2,1,0:T(8,128)(2,1)S(1)} all-to-all(bf16[4,32,2048]{2,1,0:T(8,128)(2,1)S(1)} %bitcast.79), channel_id=1, replica_groups=mesh['sp'=64,'tp'=4] {'tp'}, dimensions={0} | all-to-all | bytes 1048576 | tf_op jit(solution)/shard_map/all_to_all | solution.py:40
  (40 shorter events, 4.2 us)
Async XLA Ops:
  6.5 127.1 %copy-start = (bf16[256,2048]{1,0:T(8,128)(2,1)S(1)}, bf16[256,2048]{1,0:T(8,128)(2,1)}, u32[]{:S(2)}) copy-start(bf16[256,2048]{1,0:T(8,128)(2,1)} %param.23) | copy-start | bytes 3145732
  6.5 95.9 %all-gather.3.cloned.1.call-start = ((), (), s32[]{:S(2)}) async-start(), calls=%async_computation.2 | async-start | bytes 10649600 | tf_op jit(solution)/shard_map/all_gather | solution.py:29
  12.1 190.7 %all-gather.5.cloned.1.call-start = ((), (), s32[]{:S(2)}) async-start(), calls=%async_computation.3 | async-start | bytes 17571840 | tf_op jit(solution)/shard_map/all_gather | solution.py:18
  115.1 2.3 copy-start.3
  130.3 1.6 copy-start.1
  131.9 1.7 copy-start.5
  131.9 15.1 %copy-start.2 = (bf16[32,2048]{1,0:T(8,128)(2,1)S(1)}, bf16[32,2048]{1,0:T(8,128)(2,1)}, u32[]{:S(2)}) copy-start(bf16[32,2048]{1,0:T(8,128)(2,1)} %param.14) | copy-start | bytes 393220
  133.6 13.6 %copy-start.4 = (f32[2048]{0:T(1024)S(1)}, f32[2048]{0:T(1024)}, u32[]{:S(2)}) copy-start(f32[2048]{0:T(1024)} %param.24) | copy-start | bytes 24580
Sparse Core Ops, SparseCore 0:
  12.2 90.1 all-gather.2
  105.2 97.6 all-gather.4
where the time goes:
time: 235 us; the launch traced here: 234 us
  waiting for transfers between devices  131 us (56%)
  blocking collectives  36.7 us (16%)
  matrix products  29.5 us (13%)
  local copies, waits for them, and re-layouts  14.3 us (6%)
  between operations  13.6 us (6%)
  other arithmetic  8.62 us (4%)
    all_gather x1, waiting for transfers between devices, side_by_side(): filled = lax.all_gather(both, axis, axis=dim, tiled=True)  86.9 us
    all_gather x1, waiting for transfers between devices, turned_gather(): filled, at, done = (lax.all_gather(both, axis, axis=0, tiled=True), 0, [])  44.5 us
    all_to_all x2, blocking collectives, summed_on_arrival(): lax.all_to_all(pieces, axis, split_axis=0, concat_axis=0, tiled=True)  25.7 us
    all_gather x1, blocking collectives, on_device(): block_normed = lax.all_gather(normed, 'tp', axis=0, tiled=True)  11 us
    slice x2, local copies, waits for them, and re-layouts, on_device(): piece_keys[:, :narrow_cols].reshape(length, narrow_dev, NARROW_DIM)  8.56 us
    dot_general x1, matrix products, on_device(): jnp.dot(hidden, down_whole, preferred_element_type=jnp.float32)  7.23 us
    dot_general x2, matrix products, group_update(): jnp.einsum('hqk,khd->qhd', powers.astype(jnp.bfloat16), value_part, prefe...  5.53 us
    dot_general x2, matrix products, group_update(): jnp.einsum('qhd,kd->hqk', rotary_part, rotary_keys, preferred_element_typ...  5.16 us
  transfers between devices with their start and end apart: 2, of which 2 were waited for; matrix products, arithmetic and copies ran while one was open for 15% of the time, Pallas kernels for 0%

commit v1 on v0

--- a/solution.py
+++ b/solution.py
@@ -2,6 +2,7 @@
 import jax.numpy as jnp
 from jax import lax
 from jax.sharding import PartitionSpec as P
+from jax.lax import all_to_all, axis_size
 
 NARROW_HEADS = 8
 WIDE_HEADS = 4
@@ -15,7 +16,11 @@
 def turned_gather(arrays, axis, dims):
     turned = [jnp.moveaxis(a, dim, 0) for a, dim in zip(arrays, dims)]
     both = jnp.concatenate([t.reshape(len(t), -1) for t in turned], axis=1)
-    filled, at, done = (lax.all_gather(both, axis, axis=0, tiled=True), 0, [])
+    filled, at, done = (
+        jnp.concatenate(all_to_all(jnp.stack([both] * axis_size(axis)), axis, 0, 0), axis=0),
+        0,
+        [],
+    )
     for t, dim in zip(turned, dims):
         piece = filled[:, at : at + t[0].size].reshape(-1, *t.shape[1:])
         done.append(jnp.moveaxis(piece, 0, dim))

time: 235 us -> 577 us (2.46); the launches traced: 234 us -> 569 us
  waiting for transfers between devices: 131 us -> 463 us
  blocking collectives: 36.7 us -> 21.4 us
  starting transfers between devices: 0.04 us -> 11.5 us
    all_to_all x0 -> x2, waiting for transfers between devices: none -> 374 us  [the longest x1 365 us: turned_gather(): all_to_all(jnp.stack([both] * axis_size(axis)), axis, 0, 0)]
    all_gather x1 -> x0, waiting for transfers between devices: 44.5 us -> none  [turned_gather(): filled, at, done = (lax.all_gather(both, axis, axis=0, tiled=True), 0, [])]
    all_to_all x2 -> x1, blocking collectives: 25.7 us -> 10.3 us  [summed_on_arrival(): lax.all_to_all(pieces, axis, split_axis=0, concat_axis=0, tiled=True)]
    all_to_all x0 -> x2, starting transfers between devices: none -> 11.5 us  [the longest x1 7.5 us: turned_gather(): all_to_all(jnp.stack([both] * axis_size(axis)), axis, 0, 0)]
    another operation x2 -> x3, local copies, waits for them, and re-layouts: 0.24 us -> 6.28 us  [the longest x1 6.03 us: turned_gather(): jnp.stack([both] * axis_size(axis))]
  transfers between devices with their start and end apart: 2 -> 3, of which waited for: 2 -> 3; matrix products, arithmetic and copies ran while one was open for 15% -> 0% of each run, Pallas kernels for 0% -> 0%
where the time goes in v1:
time: 577 us; the launch traced here: 569 us
  waiting for transfers between devices  463 us (80%)
  matrix products  32.9 us (6%)
  blocking collectives  21.4 us (4%)
  local copies, waits for them, and re-layouts  19.6 us (3%)
  between operations  13.6 us (2%)
  starting transfers between devices  11.5 us (2%)
  other arithmetic  6.91 us (1%)
    all_to_all x1, waiting for transfers between devices, turned_gather(): all_to_all(jnp.stack([both] * axis_size(axis)), axis, 0, 0)  365 us
    all_gather x1, waiting for transfers between devices, side_by_side(): filled = lax.all_gather(both, axis, axis=dim, tiled=True)  88.7 us
  transfers between devices with their start and end apart: 3, of which 3 were waited for; matrix products, arithmetic and copies ran while one was open for 0% of the time, Pallas kernels for 0%

profile of v1, /device:TPU:1, one launch (start us, length us, event | category | flops | bytes accessed | tf_op | source)
XLA Modules:
  0.0 568.5 jit_solution(18373021756548918341)
XLA Ops:
  8.8 1.3 convolution_convert_fusion.1
  10.0 1.3 convolution_convert_fusion.2
  13.8 88.7 %all-gather.2.cloned.1.call-done = bf16[8192,544]{1,0:T(8,128)(2,1)} async-done(((bf16[128,544]{1,0:T(8,128)(2,1)}), bf16[8192,544]{1,0:T(8,128)(2,1)}) %all-gather.2.cloned.1.call-update) | async-done | bytes 8912912 | tf_op jit(solution)/shard_map/all_gather | solution.py:34
  102.4 2.4 convolution_bitcast_fusion.2
  104.9 3.6 fusion.91
  109.6 1.7 multiply_reduce_fusion
  111.3 3.0 fusion.90
  114.3 2.9 copy.33
  117.2 2.8 convolution_bitcast_fusion
  120.0 2.1 fusion.92
  122.2 3.5 copy-done.2
  125.7 1.1 fusion.4
  126.8 2.9 copy.36
  129.8 5.6 multiply_reduce_fusion.1
  135.4 1.2 convolution_convert_fusion
  136.6 4.0 all-to-all-start
  140.7 9.0 %all-to-all-done = bf16[4,32,2048]{2,1,0:T(8,128)(2,1)S(1)} async-done(((bf16[4,32,2048]{2,1,0:T(8,128)(2,1)}), bf16[4,32,2048]{2,1,0:T(8,128)(2,1)S(1)}, u32[]{:S(2)}, u32[]{:S(2)}) %all-to-all-start) | async-done | bytes 524320 | tf_op jit(solution)/shard_map/all_to_all | solution.py:45
  149.7 6.0 %stack.2 = bf16[64,32,4224]{2,1,0:T(8,128)(2,1)} broadcast(bf16[32,4224]{1,0:T(8,128)(2,1)S(1)} %pad_maximum_fusion), dimensions={1,2} | broadcast | bytes 17571840 | tf_op jit(solution)/shard_map/stack | solution.py:20
  155.7 7.5 %all-to-all-start.1 = ((bf16[64,32,4224]{2,1,0:T(8,128)(2,1)}), bf16[64,32,4224]{2,1,0:T(8,128)(2,1)}, u32[]{:S(2)}, u32[]{:S(2)}) async-start(bf16[64,32,4224]{2,1,0:T(8,128)(2,1)} %stack.2), calls=%async_computation.1 | async-start | bytes 34603008 | tf_op jit(solution)/shard_map/all_to_all | solution.py:20
  163.6 11.1 %all_gather.7 = bf16[128,2048]{1,0:T(8,128)(2,1)S(1)} all-gather(bf16[32,2048]{1,0:T(8,128)(2,1)S(1)} %fusion.72), channel_id=1, replica_groups=mesh['sp'=64,'tp'=4] {'tp'}, dimensions={0}, use_global_device_ids=true | all-gather | bytes 655360 | tf_op jit(solution)/shard_map/all_gather | solution.py:176
  174.7 365.0 %all-to-all-done.1 = bf16[64,32,4224]{2,1,0:T(8,128)(2,1)} async-done(((bf16[64,32,4224]{2,1,0:T(8,128)(2,1)}), bf16[64,32,4224]{2,1,0:T(8,128)(2,1)}, u32[]{:S(2)}, u32[]{:S(2)}) %all-to-all-start.1) | async-done | bytes 17301536 | tf_op jit(solution)/shard_map/all_to_all | solution.py:20
  539.7 3.6 fusion.10
  543.3 7.3 %fusion.20 = bf16[128,2048]{1,0:T(8,128)(2,1)S(1)} fusion(bf16[2048,4224]{1,0:T(8,128)(2,1)} %bitcast.23, bf16[128,2048]{1,0:T(8,128)(2,1)S(1)} %all_gather.7, f32[128,1408]{1,0:T(8,128)S(1)} %fusion.10), kind=kOutput, calls=%fused_computation.23 | convolution fusion | flops 1477738496 | bytes 13303808 | tf_op jit(solution)/shard_map/dot_general | solution.py:181
  550.6 10.3 %all_to_all.15 = bf16[4,32,2048]{2,1,0:T(8,128)(2,1)S(1)} all-to-all(bf16[4,32,2048]{2,1,0:T(8,128)(2,1)S(1)} %bitcast.81), channel_id=1, replica_groups=mesh['sp'=64,'tp'=4] {'tp'}, dimensions={0} | all-to-all | bytes 1048576 | tf_op jit(solution)/shard_map/all_to_all | solution.py:45
  (58 shorter events, 7.0 us)
Async XLA Ops:
  6.5 128.9 %copy-start = (bf16[256,2048]{1,0:T(8,128)(2,1)S(1)}, bf16[256,2048]{1,0:T(8,128)(2,1)}, u32[]{:S(2)}) copy-start(bf16[256,2048]{1,0:T(8,128)(2,1)} %param.23) | copy-start | bytes 3145732
  6.5 98.3 %copy-start.8 = (bf16[128,256]{1,0:T(8,128)(2,1)S(1)}, bf16[128,256]{1,0:T(8,128)(2,1)}, u32[]{:S(2)}) copy-start(bf16[128,256]{1,0:T(8,128)(2,1)} %param.15) | copy-start | bytes 196612
  6.5 95.9 %all-gather.2.cloned.1.call-start = ((), (), s32[]{:S(2)}) async-start(), calls=%async_computation.3 | async-start | bytes 10649600 | tf_op jit(solution)/shard_map/all_gather | solution.py:34
  102.4 7.1 %slice-start = ((s8[10485760]{0:T(1024)(128)(4,1)}), s8[4194304]{0:T(1024)(128)(4,1)S(1)}, s32[]{:S(2)}) async-start(s8[10485760]{0:T(1024)(128)(4,1)} %bitcast.77), calls=%async_computation.4 | async-start | bytes 8388608
  102.4 7.1 %slice-start.1 = ((s8[10485760]{0:T(1024)(128)(4,1)}), s8[4194304]{0:T(1024)(128)(4,1)S(1)}, s32[]{:S(2)}) async-start(s8[10485760]{0:T(1024)(128)(4,1)} %bitcast.77), calls=%async_computation.5 | async-start | bytes 8388608
  104.9 4.7 slice-start.2
  122.2 3.5 copy-start.2
  122.2 4.7 copy-start.3
  129.7 5.7 copy-start.10
  129.7 10.9 %copy-start.5 = (bf16[1408,32]{0,1:T(8,128)(2,1)S(1)}, bf16[1408,32]{0,1:T(8,128)(2,1)}, u32[]{:S(2)}) copy-start(bf16[1408,32]{0,1:T(8,128)(2,1)} %param.27) | copy-start | bytes 270340
  129.8 10.9 %copy-start.6 = (bf16[32,1408]{1,0:T(8,128)(2,1)S(1)}, bf16[32,1408]{1,0:T(8,128)(2,1)}, u32[]{:S(2)}) copy-start(bf16[32,1408]{1,0:T(8,128)(2,1)} %param.26) | copy-start | bytes 270340
  129.8 10.9 %copy-start.7 = (bf16[32,1408]{1,0:T(8,128)(2,1)S(1)}, bf16[32,1408]{1,0:T(8,128)(2,1)}, u32[]{:S(2)}) copy-start(bf16[32,1408]{1,0:T(8,128)(2,1)} %param.25) | copy-start | bytes 270340
  136.6 13.0 %all-to-all-start = ((bf16[4,32,2048]{2,1,0:T(8,128)(2,1)}), bf16[4,32,2048]{2,1,0:T(8,128)(2,1)S(1)}, u32[]{:S(2)}, u32[]{:S(2)}) async-start(bf16[4,32,2048]{2,1,0:T(8,128)(2,1)} %bitcast.21), calls=%async_computation | async-start | bytes 1048576 | tf_op jit(solution)/shard_map/all_to_all | solution.py:45
  155.7 7.6 %copy-start.4 = (bf16[32,2048]{1,0:T(8,128)(2,1)S(1)}, bf16[32,2048]{1,0:T(8,128)(2,1)}, u32[]{:S(2)}) copy-start(bf16[32,2048]{1,0:T(8,128)(2,1)} %param.14) | copy-start | bytes 393220
  155.7 7.8 %copy-start.9 = (f32[2048]{0:T(1024)S(1)}, f32[2048]{0:T(1024)}, u32[]{:S(2)}) copy-start(f32[2048]{0:T(1024)} %param.24) | copy-start | bytes 24580
  155.7 384.0 %all-to-all-start.1 = ((bf16[64,32,4224]{2,1,0:T(8,128)(2,1)}), bf16[64,32,4224]{2,1,0:T(8,128)(2,1)}, u32[]{:S(2)}, u32[]{:S(2)}) async-start(bf16[64,32,4224]{2,1,0:T(8,128)(2,1)} %stack.2), calls=%async_computation.1 | async-start | bytes 34603008 | tf_op jit(solution)/shard_map/all_to_all | solution.py:20
  543.3 18.4 %copy-start.1 = (bf16[256,2048]{1,0:T(8,128)(2,1)S(1)}, bf16[256,2048]{1,0:T(8,128)(2,1)}, u32[]{:S(2)}) copy-start(bf16[256,2048]{1,0:T(8,128)(2,1)} %param.23) | copy-start | bytes 3145732
Sparse Core Ops, SparseCore 0:
  12.2 90.1 all-gather.1
